TPU v7x, 32 devices: a whole 2x2x4 slice. The times are simulated.
32 devices in a mesh: grp: 2 (over x), ep: 4 (over y, core), tp: 4 (over z).
Axes of the slice: x: 2, y: 2, z: 4, core: 2. Of those that a mesh axis runs over, the one named last changes fastest.
Arguments:
- tokens: bfloat16 [3072, 4096], P(('grp', 'ep'), 'tp'), parts along dimension 0
- pre_gain: float32 [4096], replicated, may hold values from 0.1 to 1.9
- out_gain: float32 [4096], P('tp'), may hold values from 0.1 to 1.9
- chosen: int32 [8, 4, 48], P(('grp', 'ep')), parts along dimension 0, may hold values from 0 to 383, as said below
- route_weight: float32 [8, 4, 48], P(('grp', 'ep')), parts along dimension 0, may hold values from 0.3 to 3
- expert_gate: bfloat16 [4, 4096, 3072], P('ep', None, 'tp'), may hold values from -0.09375 to 0.09375
- expert_up: bfloat16 [4, 4096, 3072], P('ep', None, 'tp'), may hold values from -0.09375 to 0.09375
- expert_down: bfloat16 [4, 3072, 4096], P('ep', 'tp'), may hold values from -0.109375 to 0.109375
Outputs:
- output: bfloat16 [3072, 4096], P(('grp', 'ep'), 'tp'), parts along dimension 0
There are 2 independent parts, one for each index of `grp`. A program takes and returns all parts, laid end to end along the dimension named above; an argument that names none is the same for every part. Nothing has to cross between parts.
Inputs may be any that keep to these rules, and one draw needn't show every extreme that they name: chosen[b, e, k] is the position, within block b of 384 tokens, of the k-th token that expert e takes from that block; the 48 positions of one block and one expert are all different.
All inputs are finite; a program needn't handle non-finite values.
Results may differ from a plain program's by a relative error of at most 0.0075.
Values may be sent and summed in bfloat16 or wider, within the bound.
A program may use at most 64 MiB of HBM per device.

v0:
```python
import jax
import jax.numpy as jnp
from jax import lax
from jax.sharding import PartitionSpec as P

NORM_EPS = 1e-06


def shards(tokens, pre_gain, out_gain, chosen, route_weight, expert_gate, expert_up, expert_down):
    model_width = pre_gain.shape[0]
    shard_width = tokens.shape[1]
    tok_count = tokens.shape[0]
    chosen_here = chosen[0]
    experts_all = chosen_here.shape[0]
    slot_count = chosen_here.shape[1]
    resident = tokens.astype(jnp.float32)
    square_sum = lax.psum(jnp.sum(resident * resident, axis=1), "tp")
    row_scale = lax.rsqrt(square_sum / model_width + NORM_EPS)[:, None]
    gain_slice = lax.dynamic_slice_in_dim(
        pre_gain, lax.axis_index("tp") * shard_width, shard_width, 0
    )
    normed = (resident * row_scale * gain_slice).astype(jnp.bfloat16)
    outgoing = jnp.take(normed, chosen_here, axis=0)
    incoming = lax.all_to_all(outgoing, "ep", split_axis=0, concat_axis=0, tiled=True)
    picked_rows = lax.all_gather(incoming.reshape(-1, shard_width), "tp", axis=1, tiled=True)
    gate_act = jnp.dot(picked_rows, expert_gate[0], preferred_element_type=jnp.float32)
    up_act = jnp.dot(picked_rows, expert_up[0], preferred_element_type=jnp.float32)
    hidden = (jax.nn.silu(gate_act) * up_act).astype(jnp.bfloat16)
    down_shard = expert_down[0]
    summed = lax.psum_scatter(
        lax.dot_general(
            down_shard, hidden, (((0,), (1,)), ((), ())), preferred_element_type=jnp.float32
        ).astype(jnp.bfloat16),
        "tp",
        scatter_dimension=0,
        tiled=True,
    )
    expert_out = summed.reshape(shard_width, experts_all, slot_count)
    returned = lax.all_to_all(expert_out, "ep", split_axis=1, concat_axis=1, tiled=True)
    weighted = returned.astype(jnp.float32) * route_weight[0][None]
    flat_weighted = weighted.reshape(shard_width, experts_all * slot_count)
    update_cols = (
        jnp.zeros((shard_width, tok_count), jnp.float32)
        .at[:, chosen_here.reshape(-1)]
        .add(flat_weighted)
    )
    mixed_rows = resident + update_cols.T
    out_sum = lax.psum(jnp.sum(mixed_rows * mixed_rows, axis=1), "tp")
    out_scale = lax.rsqrt(out_sum / model_width + NORM_EPS)[:, None]
    return (mixed_rows * out_scale * out_gain).astype(jnp.bfloat16)


def solution(mesh):
    return jax.shard_map(
        shards,
        mesh=mesh,
        in_specs=(
            P(("grp", "ep"), "tp"),
            P(),
            P("tp"),
            P(("grp", "ep"), None, None),
            P(("grp", "ep"), None, None),
            P("ep", None, "tp"),
            P("ep", None, "tp"),
            P("ep", "tp", None),
        ),
        out_specs=P(("grp", "ep"), "tp"),
        check_vma=False,
    )
```

profile of v0, /device:TPU:0, one launch (start us, length us, event | category | flops | bytes accessed | tf_op | source)
XLA Modules:
  0.0 150.9 jit_solution(1247583569600255627)
XLA Ops:
  6.5 0.0 all-gather.2.cloned.1.call-start
  6.5 0.7 compare_select_fusion.1
  7.2 0.7 compare_and_fusion
  7.9 1.4 fusion.12
  9.3 13.5 %psum.14 = f32[384]{0:T(512)S(1)} all-reduce(f32[384]{0:T(512)S(1)} %fusion.12), channel_id=1, replica_groups=mesh['grp'=2,'ep'=4,'tp'=4] {'tp'}, use_global_device_ids=true, to_apply=%region_1.0 | all-reduce | flops 384 | bytes 3072 | tf_op jit(solution)/shard_map/psum | solution.py:17
  22.8 0.1 reshape.80
  22.9 0.7 dynamic_slice.3
  23.6 1.4 fusion.14
  24.9 1.0 gather_fusion
  26.0 0.1 broadcast_select_fusion
  26.1 10.5 %all_to_all.10 = bf16[4,48,1024]{2,1,0:T(8,128)(2,1)} all-to-all(bf16[4,48,1024]{2,1,0:T(8,128)(2,1)S(1)} %broadcast_select_fusion), channel_id=1, replica_groups=mesh['grp'=2,'ep'=4,'tp'=4] {'ep'}, dimensions={0} | all-to-all | bytes 786432 | tf_op jit(solution)/shard_map/all_to_all | solution.py:24
  36.5 0.0 all-gather.2.cloned.1.call-update
  36.6 0.0 reduce-scatter.2.cloned.1.call-start
  36.6 34.4 %all-gather.2.cloned.1.call-done = bf16[192,4096]{1,0:T(8,128)(2,1)} async-done(((bf16[192,1024]{1,0:T(8,128)(2,1)}), bf16[192,4096]{1,0:T(8,128)(2,1)}) %all-gather.2.cloned.1.call-update) | async-done | bytes 1572880 | tf_op jit(solution)/shard_map/all_gather | solution.py:25
  71.0 4.8 %fusion.4 = f32[192,768]{1,0:T(8,128)S(1)} fusion(bf16[192,4096]{1,0:T(8,128)(2,1)} %all-gather.2.cloned.1.call-done, bf16[1,4096,768]{2,1,0:T(8,128)(2,1)} %param.13), kind=kOutput, calls=%fused_computation.6 | convolution fusion | flops 1207959552 | bytes 8454144 | tf_op jit(solution)/shard_map/dot_general | solution.py:26
  75.8 0.0 copy-done.4
  75.8 9.3 %fusion.9 = bf16[4096,192]{0,1:T(8,128)(2,1)} fusion(bf16[1,768,4096]{2,1,0:T(8,128)(2,1)} %param.15, bf16[192,4096]{1,0:T(8,128)(2,1)S(1)} %copy-done.4, bf16[1,4096,768]{2,1,0:T(8,128)(2,1)} %param.14, f32[192,768]{1,0:T(8,128)S(1)} %fusion.4), kind=kOutput, calls=%fused_computation.9 | convolution fusion | flops 2417590272 | bytes 16318464 | tf_op jit(solution)/shard_map/dot_general | solution.py:31
  85.0 0.0 reduce-scatter.2.cloned.1.call-update
  85.1 34.4 %reduce-scatter.2.cloned.1.call-done = bf16[1024,192]{0,1:T(8,128)(2,1)} async-done(((bf16[4096,192]{0,1:T(8,128)(2,1)}), bf16[1024,192]{0,1:T(8,128)(2,1)}) %reduce-scatter.2.cloned.1.call-update) | async-done | bytes 393232 | tf_op jit(solution)/shard_map/reduce_scatter | solution.py:30
  119.5 3.5 %all-to-all-start.1 = ((bf16[1024,4,48]{0,2,1:T(8,128)(2,1)}), bf16[1024,4,48]{0,2,1:T(8,128)(2,1)S(1)}, u32[]{:S(2)}, u32[]{:S(2)}) async-start(bf16[1024,4,48]{0,2,1:T(8,128)(2,1)} %bitcast.48), calls=%async_computation.2 | async-start | bytes 786432 | tf_op jit(solution)/shard_map/all_to_all | solution.py:39
  123.0 0.0 copy-done.1
  123.0 0.0 copy-start
  123.0 0.1 reshape_squeeze.3
  123.1 7.3 %all-to-all-done.1 = bf16[1024,4,48]{0,2,1:T(8,128)(2,1)S(1)} async-done(((bf16[1024,4,48]{0,2,1:T(8,128)(2,1)}), bf16[1024,4,48]{0,2,1:T(8,128)(2,1)S(1)}, u32[]{:S(2)}, u32[]{:S(2)}) %all-to-all-start.1) | async-done | bytes 393248 | tf_op jit(solution)/shard_map/all_to_all | solution.py:39
  130.3 0.0 copy-done.3
  130.3 0.1 convert_multiply_fusion.2
  130.5 2.5 %scatter_custom_fusion = f32[1024,384]{0,1:T(8,128)S(1)} fusion(s32[192]{0:T(256)S(1)} %bitcast.50, f32[192,1024]{1,0:T(8,128)S(1)} %bitcast.47, f32[]{:T(128)} %constant.11.clone.1), kind=kCustom, calls=%fused_computation.21 | custom fusion | flops 196608 | bytes 1572868 | tf_op jit(solution)/shard_map/scatter-add | solution.py:45
  133.0 0.0 copy-done
  133.0 0.0 copy-start.2
  133.0 0.3 multiply_reduce_fusion
  133.3 9.6 %psum.15 = f32[384]{0:T(512)S(1)} all-reduce(f32[384]{0:T(512)S(1)} %multiply_reduce_fusion), channel_id=1, replica_groups=mesh['grp'=2,'ep'=4,'tp'=4] {'tp'}, use_global_device_ids=true, to_apply=%region_5.6 | all-reduce | flops 384 | bytes 3072 | tf_op jit(solution)/shard_map/psum | solution.py:48
  142.9 1.1 multiply_convert_fusion
  (8 shorter events, 0.0 us)
Async XLA Ops:
  6.5 64.5 %all-gather.2.cloned.1.call-start = ((), (), s32[]{:S(2)}) async-start(), calls=%async_computation.3 | async-start | bytes 1966080 | tf_op jit(solution)/shard_map/all_gather | solution.py:25
  36.6 82.9 %reduce-scatter.2.cloned.1.call-start = ((), (), s32[]{:S(2)}) async-start(), calls=%async_computation.4 | async-start | bytes 1966080 | tf_op jit(solution)/shard_map/reduce_scatter | solution.py:30
  71.0 4.8 %copy-start.4 = (bf16[192,4096]{1,0:T(8,128)(2,1)S(1)}, bf16[192,4096]{1,0:T(8,128)(2,1)}, u32[]{:S(2)}) copy-start(bf16[192,4096]{1,0:T(8,128)(2,1)} %all-gather.2.cloned.1.call-done) | copy-start | bytes 4718596
  85.0 37.9 %copy-start.1 = (s32[1,4,48]{2,1,0:T(4,128)S(1)}, s32[1,4,48]{2,1,0:T(4,128)}, u32[]{:S(2)}) copy-start(s32[1,4,48]{2,1,0:T(4,128)} %param.11) | copy-start | bytes 2308
  85.0 45.3 %copy-start.3 = (f32[1,4,48]{2,1,0:T(4,128)S(1)}, f32[1,4,48]{2,1,0:T(4,128)}, u32[]{:S(2)}) copy-start(f32[1,4,48]{2,1,0:T(4,128)} %param.12) | copy-start | bytes 2308
  119.5 10.8 %all-to-all-start.1 = ((bf16[1024,4,48]{0,2,1:T(8,128)(2,1)}), bf16[1024,4,48]{0,2,1:T(8,128)(2,1)S(1)}, u32[]{:S(2)}, u32[]{:S(2)}) async-start(bf16[1024,4,48]{0,2,1:T(8,128)(2,1)} %bitcast.48), calls=%async_computation.2 | async-start | bytes 786432 | tf_op jit(solution)/shard_map/all_to_all | solution.py:39
  123.0 10.0 %copy-start = (bf16[384,1024]{1,0:T(8,128)(2,1)S(1)}, bf16[384,1024]{1,0:T(8,128)(2,1)}, u32[]{:S(2)}) copy-start(bf16[384,1024]{1,0:T(8,128)(2,1)} %param.8) | copy-start | bytes 2359300
  133.0 9.9 %copy-start.2 = (f32[1024]{0:T(1024)S(1)}, f32[1024]{0:T(1024)}, u32[]{:S(2)}) copy-start(f32[1024]{0:T(1024)} %param.10) | copy-start | bytes 12292
Sparse Core Ops, SparseCore 0:
  36.7 34.2 all-gather.1
  85.2 34.2 reduce-scatter.1
where the time goes:
time: 151 us
  waiting for transfers between devices  76.1 us (50%)
  blocking collectives  33.6 us (22%)
  matrix products  14 us (9%)
  between operations  13.5 us (9%)
  other arithmetic  8.29 us (5%)
  starting transfers between devices  3.5 us (2%)
  local copies, waits for them, and re-layouts  1.9 us (1%)
    reduce_scatter x1, waiting for transfers between devices, shards(): lax.psum_scatter(lax.dot_general(down_shard, hidden, (((0,), (1,)), ((),...  34.4 us
    all_gather x1, waiting for transfers between devices, shards(): lax.all_gather(incoming.reshape(-1, shard_width), 'tp', axis=1, tiled=True)  34.4 us
    psum x1, blocking collectives, shards(): square_sum = lax.psum(jnp.sum(resident * resident, axis=1), 'tp')  13.5 us
    all_to_all x1, blocking collectives, shards(): lax.all_to_all(outgoing, 'ep', split_axis=0, concat_axis=0, tiled=True)  10.5 us
    psum x1, blocking collectives, shards(): out_sum = lax.psum(jnp.sum(mixed_rows * mixed_rows, axis=1), 'tp')  9.64 us
    dot_general x1, matrix products, shards(): lax.dot_general(down_shard, hidden, (((0,), (1,)), ((), ())), preferred_e...  9.25 us
    all_to_all x1, waiting for transfers between devices, shards(): lax.all_to_all(expert_out, 'ep', split_axis=1, concat_axis=1, tiled=True)  7.26 us
    dot_general x1, matrix products, shards(): jnp.dot(picked_rows, expert_gate[0], preferred_element_type=jnp.float32)  4.76 us
  transfers between devices with their start and end apart: 3, of which 3 were waited for; matrix products, arithmetic and copies ran while one was open for 0% of the time, Pallas kernels for 0%

commit v1 on v0

v1 whole, which is shorter than its diff:
```python
import functools

import jax
import jax.numpy as jnp
from jax import lax
from jax.experimental import pallas as pl
from jax.experimental.pallas import tpu as pltpu
from jax.sharding import PartitionSpec as P

NORM_EPS = 1e-06
MESH = pl.DeviceIdType.MESH
LANES = 128


def both(*conditions):
    held = conditions[0]
    for condition in conditions[1:]:
        held = jnp.logical_and(held, condition)
    return held


def line_order(place, count, step):
    near = jnp.minimum(place, count - 1 - place)
    reach = (step + 1) // 2
    inner = jnp.where(step % 2 == 1, place - reach, place + reach)
    outer = jnp.where(place < count - 1 - place, step, count - 1 - step)
    return jnp.where(step <= 2 * near, inner, outer)


def pair_of(here, count, chunk, sign):
    chips = count // 2
    chip, core = here // 2, here % 2
    far_chip = (chip + sign * ((chunk - 1) // 2 + 1) + 2 * chips) % chips
    far_core = jnp.where((chunk - 1) % 2 == 0, core, 1 - core)
    far = far_chip * 2 + far_core
    far = jnp.where(chunk == count - 1, chip * 2 + 1 - core, far)
    return jnp.where(chunk == 0, here, far)


def layer_kernel(
    n_ep, n_tp, model_width,
    tokens_ref, pre_gain_ref, out_gain_ref, chosen_ref, weight_ref, gate_hbm, up_hbm, down_hbm,
    out_ref,
    gate_w, up_w, down_w, rows, picked, part, carried, landed, gate_acc, up_acc, square_acc, hidden_ref,
    leaving, returned, mixed, sums_out, sums_in,
    gate_sem, up_sem, down_sem, pick_send, pick_recv, row_send, row_recv, part_send, part_recv,
    back_send, back_recv, sum_send, sum_recv,
):
    grp, me, at = lax.axis_index("grp"), lax.axis_index("ep"), lax.axis_index("tp")
    tok_count, width = tokens_ref.shape
    slots = chosen_ref.shape[2]
    last = n_tp - 1

    barrier = pltpu.get_barrier_semaphore()
    for step in range(1, n_tp):
        pl.semaphore_signal(barrier, inc=1, device_id=(grp, me, (at + step) % n_tp), device_id_type=MESH)
    for step in range(1, n_ep):
        pl.semaphore_signal(barrier, inc=1, device_id=(grp, (me + step) % n_ep, at), device_id_type=MESH)

    def load_gate(s):
        return pltpu.make_async_copy(gate_hbm.at[0, pl.ds(pl.multiple_of(s * width, width), width)], gate_w.at[s], gate_sem.at[s])

    def load_up(s):
        return pltpu.make_async_copy(up_hbm.at[0, pl.ds(pl.multiple_of(s * width, width), width)], up_w.at[s], up_sem.at[s])

    def load_down(s):
        return pltpu.make_async_copy(down_hbm.at[0, :, pl.ds(pl.multiple_of(s * width, width), width)], down_w.at[s], down_sem.at[s])

    @pl.loop(0, n_tp)
    def _(step):
        s = line_order(at, n_tp, step)
        load_gate(s).start()
        load_up(s).start()

    @pl.loop(0, n_tp)
    def _(step):
        load_down(line_order(at, n_tp, last - step)).start()

    def remote(src, dst, send, recv, ep_index, tp_index):
        return pltpu.make_async_remote_copy(
            src_ref=src, dst_ref=dst, send_sem=send, recv_sem=recv,
            device_id=(grp, ep_index, tp_index), device_id_type=MESH,
        )

    def pick_copy(c):
        return remote(picked.at[c], rows.at[c, at], pick_send.at[c], pick_recv.at[c], pair_of(me, n_ep, c, -1), at)

    def row_copy(c, s, right):
        return remote(
            rows.at[c, s], rows.at[c, s], row_send.at[right, c, s], row_recv.at[c, s],
            me, jnp.clip(at + (2 * right - 1), 0, last),
        )

    def part_copy(c, d, right):
        return remote(
            carried.at[c, d], landed.at[1 - right, c, d], part_send.at[c, d], part_recv.at[1 - right, c, d],
            me, jnp.clip(at + (2 * right - 1), 0, last),
        )

    def part_wait(c, d, side):
        remote(carried.at[c, d], landed.at[side, c, d], part_send.at[c, d], part_recv.at[side, c, d],
               me, jnp.clip(at + (2 * side - 1), 0, last)).wait_recv()

    def back_copy(c):
        return remote(leaving.at[c], returned.at[c], back_send.at[c], back_recv.at[c], pair_of(me, n_ep, c, 1), at)

    def sum_copy(step):
        return remote(sums_out, sums_in.at[at], sum_send.at[step], sum_recv.at[at], me, (at + step) % n_tp)

    place_of = lax.broadcasted_iota(jnp.int32, (tok_count, slots), 0)

    def pick(c):
        expert = pair_of(me, n_ep, c, -1)
        one_hot = jnp.where(place_of == chosen_ref[0, pl.ds(expert, 1), :], 1.0, 0.0).astype(jnp.bfloat16)
        return lax.dot_general(
            one_hot, tokens_ref[...], (((0,), (0,)), ((), ())), preferred_element_type=jnp.float32
        ).astype(jnp.bfloat16)

    def send_row(c, s):
        @pl.when(both(s <= at, at < last))
        def _():
            row_copy(c, s, 1).start()

        @pl.when(both(s >= at, at > 0))
        def _():
            row_copy(c, s, 0).start()

    rows[0, at] = pick(0)
    pl.semaphore_wait(barrier, n_tp - 1 + n_ep - 1)
    send_row(0, at)

    @pl.loop(1, n_ep)
    def _(c):
        picked[c] = pick(c)
        pick_copy(c).start()

    mixed[...] = tokens_ref[...].astype(jnp.float32)

    def multiply(c, step):
        s = line_order(at, n_tp, step)

        @pl.when(step > 0)
        def _():
            row_copy(c, s, 1).wait_recv()
            send_row(c, s)

        @pl.when(c == 0)
        def _():
            load_gate(s).wait()
            load_up(s).wait()

        raw = rows[c, s].astype(jnp.float32)
        scaled = (raw * pre_gain_ref[:, pl.ds(pl.multiple_of(s * width, width), width)]).astype(jnp.bfloat16)
        gate_acc[...] += jnp.dot(scaled, gate_w[s], preferred_element_type=jnp.float32)
        up_acc[...] += jnp.dot(scaled, up_w[s], preferred_element_type=jnp.float32)
        square_acc[...] += jnp.sum(raw * raw, axis=1, keepdims=True)

    def first_hop(d):
        return jnp.logical_or(both(at == 0, d > at), both(at == last, d < at))

    def start_part(c, d):
        @pl.when(d > at)
        def _():
            part_copy(c, d, 1).start()

        @pl.when(d < at)
        def _():
            part_copy(c, d, 0).start()

    def project(c, step):
        d = line_order(at, n_tp, last - step)

        @pl.when(c == 0)
        def _():
            load_down(d).wait()

        term = jnp.dot(hidden_ref[...], down_w[d], preferred_element_type=jnp.float32)
        part[c, d] = term

        @pl.when(first_hop(d))
        def _():
            carried[c, d] = part[c, d].astype(jnp.bfloat16)
            start_part(c, d)

    def relay(c):
        @pl.loop(0, last)
        def _(step):
            d = line_order(at, n_tp, last - step)

            @pl.when(jnp.logical_not(first_hop(d)))
            def _():
                side = jnp.where(d > at, 0, 1)
                part_wait(c, d, side)
                carried[c, d] = (part[c, d] + landed[side, c, d].astype(jnp.float32)).astype(jnp.bfloat16)
                start_part(c, d)

    def finish(c):
        @pl.when(at > 0)
        def _():
            part_wait(c, at, 0)
            part[c, at] += landed[0, c, at].astype(jnp.float32)

        @pl.when(at < last)
        def _():
            part_wait(c, at, 1)
            part[c, at] += landed[1, c, at].astype(jnp.float32)

        @pl.when(c == 0)
        def _():
            returned[0] = part[0, at].astype(jnp.bfloat16)

        @pl.when(c > 0)
        def _():
            leaving[c] = part[c, at].astype(jnp.bfloat16)
            back_copy(c).start()

    def scatter(c):
        @pl.when(c > 0)
        def _():
            back_copy(c).wait_recv()

        expert = pair_of(me, n_ep, c, -1)
        weight = weight_ref[0, pl.ds(expert, 1), :]
        coarse = weight.astype(jnp.bfloat16).astype(jnp.float32)
        here = place_of == chosen_ref[0, pl.ds(expert, 1), :]
        spread = jnp.where(here, coarse, 0.0).astype(jnp.bfloat16)
        fine = jnp.where(here, weight - coarse, 0.0).astype(jnp.bfloat16)
        block = returned[c]
        mixed[...] += jnp.dot(spread, block, preferred_element_type=jnp.float32) + jnp.dot(
            fine, block, preferred_element_type=jnp.float32
        )

    @pl.loop(0, n_ep)
    def _(c):
        gate_acc[...] = jnp.zeros_like(gate_acc)
        up_acc[...] = jnp.zeros_like(up_acc)
        square_acc[...] = jnp.zeros_like(square_acc)

        @pl.loop(0, n_tp)
        def _(step):
            multiply(c, step)

            @pl.when(both(step == 0, c + 1 < n_ep))
            def _():
                pick_copy(c + 1).wait_recv()
                send_row(c + 1, at)

        scale = lax.rsqrt(square_acc[...] / model_width + NORM_EPS)
        gate = gate_acc[...] * scale
        hidden_ref[...] = (gate / (1.0 + jnp.exp(-gate)) * (up_acc[...] * scale)).astype(jnp.bfloat16)

        @pl.loop(0, n_tp)
        def _(step):
            project(c, step)

        @pl.when(c >= 1)
        def _():
            relay(c - 1)

        @pl.when(c >= 2)
        def _():
            finish(c - 2)

    if n_ep >= 2:
        finish(n_ep - 2)

    @pl.loop(0, n_ep - 2)
    def _(c):
        scatter(c)

    relay(n_ep - 1)
    if n_ep >= 2:
        scatter(n_ep - 2)
    finish(n_ep - 1)
    scatter(n_ep - 1)

    square = mixed[...] * mixed[...]
    lanes = square[:, :LANES]
    for k in range(1, width // LANES):
        lanes = lanes + square[:, k * LANES:(k + 1) * LANES]
    mine = jnp.sum(lanes.T, axis=0, keepdims=True)
    sums_out[...] = jnp.broadcast_to(mine, sums_out.shape)
    for step in range(1, n_tp):
        sum_copy(step).start()
    total = sums_out[...]
    for step in range(1, n_tp):
        source = (at + step) % n_tp
        remote(sums_out, sums_in.at[source], sum_send.at[step], sum_recv.at[source], me, source).wait_recv()
        total = total + sums_in[source]
    scale = lax.rsqrt(total / model_width + NORM_EPS)
    column = jnp.concatenate([scale] * (LANES // scale.shape[0]), axis=0).T
    for k in range(width // LANES):
        span = slice(k * LANES, (k + 1) * LANES)
        out_ref[:, span] = (mixed[:, span] * column * out_gain_ref[:, span]).astype(out_ref.dtype)

    for step in range(1, n_tp):
        sum_copy(step).wait_send()

    @pl.loop(0, n_ep)
    def _(c):
        @pl.when(c > 0)
        def _():
            pick_copy(c).wait_send()
            back_copy(c).wait_send()

        @pl.loop(0, n_tp)
        def _(s):
            @pl.when(both(s <= at, at < last))
            def _():
                row_copy(c, s, 1).wait_send()

            @pl.when(both(s >= at, at > 0))
            def _():
                row_copy(c, s, 0).wait_send()

            @pl.when(s > at)
            def _():
                part_copy(c, s, 1).wait_send()

            @pl.when(s < at)
            def _():
                part_copy(c, s, 0).wait_send()


def solution(mesh):
    n_ep, n_tp = mesh.shape["ep"], mesh.shape["tp"]

    def shards(tokens, pre_gain, out_gain, chosen, route_weight, expert_gate, expert_up, expert_down):
        tok_count, width = tokens.shape
        model_width = pre_gain.shape[0]
        slots, units = chosen.shape[2], expert_gate.shape[2]
        bf16, f32 = jnp.bfloat16, jnp.float32
        dma = pltpu.SemaphoreType.DMA
        vmem = pl.BlockSpec(memory_space=pltpu.VMEM)
        hbm = pl.BlockSpec(memory_space=pl.ANY)
        return pl.pallas_call(
            functools.partial(layer_kernel, n_ep, n_tp, model_width),
            out_shape=jax.ShapeDtypeStruct((tok_count, width), bf16),
            in_specs=[vmem] * 5 + [hbm] * 3,
            out_specs=vmem,
            scratch_shapes=[
                pltpu.VMEM((n_tp, width, units), bf16),
                pltpu.VMEM((n_tp, width, units), bf16),
                pltpu.VMEM((n_tp, units, width), bf16),
                pltpu.VMEM((n_ep, n_tp, slots, width), bf16),
                pltpu.VMEM((n_ep, slots, width), bf16),
                pltpu.VMEM((n_ep, n_tp, slots, width), f32),
                pltpu.VMEM((n_ep, n_tp, slots, width), bf16),
                pltpu.VMEM((2, n_ep, n_tp, slots, width), bf16),
                pltpu.VMEM((slots, units), f32),
                pltpu.VMEM((slots, units), f32),
                pltpu.VMEM((slots, 1), f32),
                pltpu.VMEM((slots, units), bf16),
                pltpu.VMEM((n_ep, slots, width), bf16),
                pltpu.VMEM((n_ep, slots, width), bf16),
                pltpu.VMEM((tok_count, width), f32),
                pltpu.VMEM((8, tok_count), f32),
                pltpu.VMEM((n_tp, 8, tok_count), f32),
                dma((n_tp,)), dma((n_tp,)), dma((n_tp,)),
                dma((n_ep,)), dma((n_ep,)),
                dma((2, n_ep, n_tp)), dma((n_ep, n_tp)),
                dma((n_ep, n_tp)), dma((2, n_ep, n_tp)),
                dma((n_ep,)), dma((n_ep,)),
                dma((n_tp,)), dma((n_tp,)),
            ],
            compiler_params=pltpu.CompilerParams(
                collective_id=0, has_side_effects=True, vmem_limit_bytes=67043328
            ),
        )(
            tokens, pre_gain.reshape(1, -1), out_gain.reshape(1, -1), chosen, route_weight,
            expert_gate, expert_up, expert_down,
        )

    return jax.shard_map(
        shards,
        mesh=mesh,
        in_specs=(
            P(("grp", "ep"), "tp"),
            P(),
            P("tp"),
            P(("grp", "ep"), None, None),
            P(("grp", "ep"), None, None),
            P("ep", None, "tp"),
            P("ep", None, "tp"),
            P("ep", "tp", None),
        ),
        out_specs=P(("grp", "ep"), "tp"),
        check_vma=False,
    )
```

time: 151 us -> 77.3 us (0.51)
  waiting for transfers between devices: 76.1 us -> 0 us
  Pallas kernels: 0 us -> 75.1 us
  blocking collectives: 33.6 us -> 0 us
  matrix products: 14 us -> 0 us
  between operations: 13.5 us -> 0.01 us
  other arithmetic: 8.29 us -> 0 us
  starting transfers between devices: 3.5 us -> 0 us
    pallas_call x0 -> x1, Pallas kernels: none -> 75.1 us  [shards(): pl.pallas_call(functools.partial(layer_kernel, n_ep, n_tp, model_width),...]
    reduce_scatter x1 -> x0, waiting for transfers between devices: 34.4 us -> none  [shards(): lax.psum_scatter(lax.dot_general(down_shard, hidden, (((0,), (1,)), ((),...]
    all_gather x1 -> x0, waiting for transfers between devices: 34.4 us -> none  [shards(): lax.all_gather(incoming.reshape(-1, shard_width), 'tp', axis=1, tiled=True)]
    psum x2 -> x0, blocking collectives: 23.1 us -> none  [the longest x1 13.5 us: shards(): square_sum = lax.psum(jnp.sum(resident * resident, axis=1), 'tp')]
    dot_general x2 -> x0, matrix products: 14 us -> none  [the longest x1 9.25 us: shards(): lax.dot_general(down_shard, hidden, (((0,), (1,)), ((), ())), preferred_e...]
    all_to_all x1 -> x0, blocking collectives: 10.5 us -> none  [shards(): lax.all_to_all(outgoing, 'ep', split_axis=0, concat_axis=0, tiled=True)]
    all_to_all x1 -> x0, waiting for transfers between devices: 7.26 us -> none  [shards(): lax.all_to_all(expert_out, 'ep', split_axis=1, concat_axis=1, tiled=True)]
    all_to_all x1 -> x0, starting transfers between devices: 3.46 us -> none  [shards(): lax.all_to_all(expert_out, 'ep', split_axis=1, concat_axis=1, tiled=True)]
  transfers between devices with their start and end apart: 3 -> 0, of which waited for: 3 -> 0; matrix products, arithmetic and copies ran while one was open for 0% -> 0% of each run, Pallas kernels for 0% -> 0%
where the time goes in v1:
time: 77.3 us; the launch traced here: 77.2 us
  Pallas kernels  75.1 us (97%)
  local copies, waits for them, and re-layouts  2.06 us (3%)
    pallas_call x1, Pallas kernels, shards(): pl.pallas_call(functools.partial(layer_kernel, n_ep, n_tp, model_width),...  75.1 us
    unnamed x1, local copies, waits for them, and re-layouts  2.06 us

profile of v1, /device:TPU:0, one launch (start us, length us, event | category | flops | bytes accessed | tf_op | source)
XLA Modules:
  0.0 77.2 jit_solution(12854137331137017075)
XLA Ops:
  0.0 75.1 %shard_map.82 = bf16[384,1024]{1,0:T(8,128)(2,1)} custom-call(bf16[384,1024]{1,0:T(8,128)(2,1)} %tokens_ref.1, f32[1,4096]{1,0:T(1,128)} %bitcast.2, f32[1,1024]{1,0:T(1,128)} %bitcast.3, s32[1,4,48]{2,1,0:T(4,128)} %chosen_ref.1, f32[1,4,48]{2,1,0:T(4,128)} %weight_ref.1, bf16[1,4096,768]{2,1,0:T(8,128)(2,1)} %gate_hbm.1, bf16[1,4096,768]{2,1,0:T(8,128)(2,1)} %up_hbm.1, ...), custom_call_target="tpu_custom_call" | custom-call | tf_op jit(solution)/shard_map/pallas_call | solution.py:336
  75.1 2.1 %copy.10 = bf16[384,1024]{1,0:T(8,128)(2,1)} copy(bf16[384,1024]{1,0:T(8,128)(2,1)} %shard_map.82) | data formatting | bytes 1572864

commit v2 on v1

--- a/solution.py
+++ b/solution.py
@@ -10,6 +10,7 @@
 NORM_EPS = 1e-06
 MESH = pl.DeviceIdType.MESH
 LANES = 128
+PIECES = 2
 
 
 def both(*conditions):
@@ -50,6 +51,7 @@
     tok_count, width = tokens_ref.shape
     slots = chosen_ref.shape[2]
     last = n_tp - 1
+    pieces, narrow = down_w.shape[1], down_w.shape[3]
 
     barrier = pltpu.get_barrier_semaphore()
     for step in range(1, n_tp):
@@ -63,8 +65,9 @@
     def load_up(s):
         return pltpu.make_async_copy(up_hbm.at[0, pl.ds(pl.multiple_of(s * width, width), width)], up_w.at[s], up_sem.at[s])
 
-    def load_down(s):
-        return pltpu.make_async_copy(down_hbm.at[0, :, pl.ds(pl.multiple_of(s * width, width), width)], down_w.at[s], down_sem.at[s])
+    def load_down(s, h):
+        span = pl.ds(pl.multiple_of((s * pieces + h) * narrow, narrow), narrow)
+        return pltpu.make_async_copy(down_hbm.at[0, :, span], down_w.at[s, h], down_sem.at[s, h])
 
     @pl.loop(0, n_tp)
     def _(step):
@@ -74,7 +77,8 @@
 
     @pl.loop(0, n_tp)
     def _(step):
-        load_down(line_order(at, n_tp, last - step)).start()
+        for h in range(pieces):
+            load_down(line_order(at, n_tp, last - step), h).start()
 
     def remote(src, dst, send, recv, ep_index, tp_index):
         return pltpu.make_async_remote_copy(
@@ -91,18 +95,21 @@
             me, jnp.clip(at + (2 * right - 1), 0, last),
         )
 
-    def part_copy(c, d, right):
+    def part_copy(c, d, h, right):
         return remote(
-            carried.at[c, d], landed.at[1 - right, c, d], part_send.at[c, d], part_recv.at[1 - right, c, d],
+            carried.at[c, d, h], landed.at[1 - right, c, d, h],
+            part_send.at[c, d, h], part_recv.at[1 - right, c, d, h],
             me, jnp.clip(at + (2 * right - 1), 0, last),
         )
 
-    def part_wait(c, d, side):
-        remote(carried.at[c, d], landed.at[side, c, d], part_send.at[c, d], part_recv.at[side, c, d],
+    def part_wait(c, d, h, side):
+        remote(carried.at[c, d, h], landed.at[side, c, d, h], part_send.at[c, d, h], part_recv.at[side, c, d, h],
                me, jnp.clip(at + (2 * side - 1), 0, last)).wait_recv()
 
-    def back_copy(c):
-        return remote(leaving.at[c], returned.at[c], back_send.at[c], back_recv.at[c], pair_of(me, n_ep, c, 1), at)
+    def back_copy(c, h):
+        return remote(
+            leaving.at[c, h], returned.at[c, h], back_send.at[c, h], back_recv.at[c, h], pair_of(me, n_ep, c, 1), at
+        )
 
     def sum_copy(step):
         return remote(sums_out, sums_in.at[at], sum_send.at[step], sum_recv.at[at], me, (at + step) % n_tp)
@@ -136,13 +143,23 @@
 
     mixed[...] = tokens_ref[...].astype(jnp.float32)
 
+    def pass_on(slot):
+        @pl.when(both(slot % n_tp > 0, slot < n_ep * n_tp))
+        def _():
+            c = slot // n_tp
+            s = line_order(at, n_tp, slot % n_tp)
+            row_copy(c, s, 1).wait_recv()
+            send_row(c, s)
+
+    def start_own(slot):
+        @pl.when(both(slot % n_tp == 0, slot < n_ep * n_tp))
+        def _():
+            c = slot // n_tp
+            pick_copy(c).wait_recv()
+            send_row(c, at)
+
     def multiply(c, step):
         s = line_order(at, n_tp, step)
-
-        @pl.when(step > 0)
-        def _():
-            row_copy(c, s, 1).wait_recv()
-            send_row(c, s)
 
         @pl.when(c == 0)
         def _():
@@ -158,77 +175,84 @@
     def first_hop(d):
         return jnp.logical_or(both(at == 0, d > at), both(at == last, d < at))
 
-    def start_part(c, d):
+    def start_part(c, d, h):
         @pl.when(d > at)
         def _():
-            part_copy(c, d, 1).start()
+            part_copy(c, d, h, 1).start()
 
         @pl.when(d < at)
         def _():
-            part_copy(c, d, 0).start()
+            part_copy(c, d, h, 0).start()
 
     def project(c, step):
         d = line_order(at, n_tp, last - step)
 
-        @pl.when(c == 0)
-        def _():
-            load_down(d).wait()
-
-        term = jnp.dot(hidden_ref[...], down_w[d], preferred_element_type=jnp.float32)
-        part[c, d] = term
-
-        @pl.when(first_hop(d))
-        def _():
-            carried[c, d] = part[c, d].astype(jnp.bfloat16)
-            start_part(c, d)
-
-    def relay(c):
+        for h in range(pieces):
+            @pl.when(c == 0)
+            def _():
+                load_down(d, h).wait()
+
+            part[c, d, h] = jnp.dot(hidden_ref[...], down_w[d, h], preferred_element_type=jnp.float32)
+
+            @pl.when(first_hop(d))
+            def _():
+                carried[c, d, h] = part[c, d, h].astype(jnp.bfloat16)
+                start_part(c, d, h)
+
+    def second_hop(d):
+        return jnp.logical_or(both(at == 1, d > at), both(at == last - 1, d < at))
+
+    def relay(c, early):
         @pl.loop(0, last)
         def _(step):
             d = line_order(at, n_tp, last - step)
-
-            @pl.when(jnp.logical_not(first_hop(d)))
+            wanted = second_hop(d) if early else jnp.logical_not(second_hop(d))
+
+            @pl.when(both(wanted, jnp.logical_not(first_hop(d))))
             def _():
                 side = jnp.where(d > at, 0, 1)
-                part_wait(c, d, side)
-                carried[c, d] = (part[c, d] + landed[side, c, d].astype(jnp.float32)).astype(jnp.bfloat16)
-                start_part(c, d)
+                for h in range(pieces):
+                    part_wait(c, d, h, side)
+                    carried[c, d, h] = (part[c, d, h] + landed[side, c, d, h].astype(jnp.float32)).astype(jnp.bfloat16)
+                    start_part(c, d, h)
 
     def finish(c):
-        @pl.when(at > 0)
-        def _():
-            part_wait(c, at, 0)
-            part[c, at] += landed[0, c, at].astype(jnp.float32)
-
-        @pl.when(at < last)
-        def _():
-            part_wait(c, at, 1)
-            part[c, at] += landed[1, c, at].astype(jnp.float32)
-
-        @pl.when(c == 0)
-        def _():
-            returned[0] = part[0, at].astype(jnp.bfloat16)
-
-        @pl.when(c > 0)
-        def _():
-            leaving[c] = part[c, at].astype(jnp.bfloat16)
-            back_copy(c).start()
+        for h in range(pieces):
+            @pl.when(at > 0)
+            def _():
+                part_wait(c, at, h, 0)
+                part[c, at, h] += landed[0, c, at, h].astype(jnp.float32)
+
+            @pl.when(at < last)
+            def _():
+                part_wait(c, at, h, 1)
+                part[c, at, h] += landed[1, c, at, h].astype(jnp.float32)
+
+            @pl.when(c == 0)
+            def _():
+                returned[0, h] = part[0, at, h].astype(jnp.bfloat16)
+
+            @pl.when(c > 0)
+            def _():
+                leaving[c, h] = part[c, at, h].astype(jnp.bfloat16)
+                back_copy(c, h).start()
 
     def scatter(c):
-        @pl.when(c > 0)
-        def _():
-            back_copy(c).wait_recv()
-
         expert = pair_of(me, n_ep, c, -1)
         weight = weight_ref[0, pl.ds(expert, 1), :]
         coarse = weight.astype(jnp.bfloat16).astype(jnp.float32)
         here = place_of == chosen_ref[0, pl.ds(expert, 1), :]
         spread = jnp.where(here, coarse, 0.0).astype(jnp.bfloat16)
         fine = jnp.where(here, weight - coarse, 0.0).astype(jnp.bfloat16)
-        block = returned[c]
-        mixed[...] += jnp.dot(spread, block, preferred_element_type=jnp.float32) + jnp.dot(
-            fine, block, preferred_element_type=jnp.float32
-        )
+        for h in range(pieces):
+            @pl.when(c > 0)
+            def _():
+                back_copy(c, h).wait_recv()
+
+            block = returned[c, h]
+            mixed[:, h * narrow:(h + 1) * narrow] += jnp.dot(
+                spread, block, preferred_element_type=jnp.float32
+            ) + jnp.dot(fine, block, preferred_element_type=jnp.float32)
 
     @pl.loop(0, n_ep)
     def _(c):
@@ -238,12 +262,14 @@
 
         @pl.loop(0, n_tp)
         def _(step):
+            slot = c * n_tp + step
+            pass_on(slot)
             multiply(c, step)
-
-            @pl.when(both(step == 0, c + 1 < n_ep))
-            def _():
-                pick_copy(c + 1).wait_recv()
-                send_row(c + 1, at)
+            start_own(slot + n_tp + 1)
+
+            @pl.when(slot == 0)
+            def _():
+                start_own(n_tp)
 
         scale = lax.rsqrt(square_acc[...] / model_width + NORM_EPS)
         gate = gate_acc[...] * scale
@@ -255,22 +281,24 @@
 
         @pl.when(c >= 1)
         def _():
-            relay(c - 1)
-
-        @pl.when(c >= 2)
-        def _():
-            finish(c - 2)
-
-    if n_ep >= 2:
-        finish(n_ep - 2)
-
-    @pl.loop(0, n_ep - 2)
+            relay(c - 1, True)
+
+    @pl.loop(0, n_ep - 1)
+    def _(c):
+        relay(c, False)
+
+    relay(n_ep - 1, True)
+
+    @pl.loop(0, n_ep - 1)
+    def _(c):
+        finish(c)
+
+    relay(n_ep - 1, False)
+
+    @pl.loop(0, n_ep - 1)
     def _(c):
         scatter(c)
 
-    relay(n_ep - 1)
-    if n_ep >= 2:
-        scatter(n_ep - 2)
     finish(n_ep - 1)
     scatter(n_ep - 1)
 
@@ -301,7 +329,8 @@
         @pl.when(c > 0)
         def _():
             pick_copy(c).wait_send()
-            back_copy(c).wait_send()
+            for h in range(pieces):
+                back_copy(c, h).wait_send()
 
         @pl.loop(0, n_tp)
         def _(s):
@@ -313,13 +342,14 @@
             def _():
                 row_copy(c, s, 0).wait_send()
 
-            @pl.when(s > at)
-            def _():
-                part_copy(c, s, 1).wait_send()
-
-            @pl.when(s < at)
-            def _():
-                part_copy(c, s, 0).wait_send()
+            for h in range(pieces):
+                @pl.when(s > at)
+                def _():
+                    part_copy(c, s, h, 1).wait_send()
+
+                @pl.when(s < at)
+                def _():
+                    part_copy(c, s, h, 0).wait_send()
 
 
 def solution(mesh):
@@ -329,6 +359,7 @@
         tok_count, width = tokens.shape
         model_width = pre_gain.shape[0]
         slots, units = chosen.shape[2], expert_gate.shape[2]
+        narrow = width // PIECES
         bf16, f32 = jnp.bfloat16, jnp.float32
         dma = pltpu.SemaphoreType.DMA
         vmem = pl.BlockSpec(memory_space=pltpu.VMEM)
@@ -341,26 +372,26 @@
             scratch_shapes=[
                 pltpu.VMEM((n_tp, width, units), bf16),
                 pltpu.VMEM((n_tp, width, units), bf16),
-                pltpu.VMEM((n_tp, units, width), bf16),
+                pltpu.VMEM((n_tp, PIECES, units, narrow), bf16),
                 pltpu.VMEM((n_ep, n_tp, slots, width), bf16),
                 pltpu.VMEM((n_ep, slots, width), bf16),
-                pltpu.VMEM((n_ep, n_tp, slots, width), f32),
-                pltpu.VMEM((n_ep, n_tp, slots, width), bf16),
-                pltpu.VMEM((2, n_ep, n_tp, slots, width), bf16),
+                pltpu.VMEM((n_ep, n_tp, PIECES, slots, narrow), f32),
+                pltpu.VMEM((n_ep, n_tp, PIECES, slots, narrow), bf16),
+                pltpu.VMEM((2, n_ep, n_tp, PIECES, slots, narrow), bf16),
                 pltpu.VMEM((slots, units), f32),
                 pltpu.VMEM((slots, units), f32),
                 pltpu.VMEM((slots, 1), f32),
                 pltpu.VMEM((slots, units), bf16),
-                pltpu.VMEM((n_ep, slots, width), bf16),
-                pltpu.VMEM((n_ep, slots, width), bf16),
+                pltpu.VMEM((n_ep, PIECES, slots, narrow), bf16),
+                pltpu.VMEM((n_ep, PIECES, slots, narrow), bf16),
                 pltpu.VMEM((tok_count, width), f32),
                 pltpu.VMEM((8, tok_count), f32),
                 pltpu.VMEM((n_tp, 8, tok_count), f32),
-                dma((n_tp,)), dma((n_tp,)), dma((n_tp,)),
+                dma((n_tp,)), dma((n_tp,)), dma((n_tp, PIECES)),
                 dma((n_ep,)), dma((n_ep,)),
                 dma((2, n_ep, n_tp)), dma((n_ep, n_tp)),
-                dma((n_ep, n_tp)), dma((2, n_ep, n_tp)),
-                dma((n_ep,)), dma((n_ep,)),
+                dma((n_ep, n_tp, PIECES)), dma((2, n_ep, n_tp, PIECES)),
+                dma((n_ep, PIECES)), dma((n_ep, PIECES)),
                 dma((n_tp,)), dma((n_tp,)),
             ],
             compiler_params=pltpu.CompilerParams(

time: 77.3 us -> 67.8 us (0.88)
  Pallas kernels: 75.1 us -> 65.6 us
    pallas_call x1, Pallas kernels: 75.1 us -> 65.6 us  [shards(): pl.pallas_call(functools.partial(layer_kernel, n_ep, n_tp, model_width),...]
where the time goes in v2:
time: 67.8 us; the launch traced here: 67.7 us
  Pallas kernels  65.6 us (97%)
  local copies, waits for them, and re-layouts  2.06 us (3%)
    pallas_call x1, Pallas kernels, shards(): pl.pallas_call(functools.partial(layer_kernel, n_ep, n_tp, model_width),...  65.6 us
    unnamed x1, local copies, waits for them, and re-layouts  2.06 us

profile of v2, /device:TPU:0, one launch (start us, length us, event | category | flops | bytes accessed | tf_op | source)
XLA Modules:
  0.0 67.7 jit_solution(4759294932379042952)
XLA Ops:
  0.0 65.6 %shard_map.82 = bf16[384,1024]{1,0:T(8,128)(2,1)} custom-call(bf16[384,1024]{1,0:T(8,128)(2,1)} %tokens_ref.1, f32[1,4096]{1,0:T(1,128)} %bitcast.2, f32[1,1024]{1,0:T(1,128)} %bitcast.3, s32[1,4,48]{2,1,0:T(4,128)} %chosen_ref.1, f32[1,4,48]{2,1,0:T(4,128)} %weight_ref.1, bf16[1,4096,768]{2,1,0:T(8,128)(2,1)} %gate_hbm.1, bf16[1,4096,768]{2,1,0:T(8,128)(2,1)} %up_hbm.1, ...), custom_call_target="tpu_custom_call" | custom-call | tf_op jit(solution)/shard_map/pallas_call | solution.py:367
  65.6 2.1 %copy.10 = bf16[384,1024]{1,0:T(8,128)(2,1)} copy(bf16[384,1024]{1,0:T(8,128)(2,1)} %shard_map.82) | data formatting | bytes 1572864

commit v3 on v2

--- a/solution.py
+++ b/solution.py
@@ -10,7 +10,7 @@
 NORM_EPS = 1e-06
 MESH = pl.DeviceIdType.MESH
 LANES = 128
-PIECES = 2
+PIECES = 1
 
 
 def both(*conditions):
@@ -279,9 +279,11 @@
         def _(step):
             project(c, step)
 
-        @pl.when(c >= 1)
-        def _():
-            relay(c - 1, True)
+        @pl.when(c >= 2)
+        def _():
+            relay(c - 2, True)
+
+    relay(n_ep - 2, True)
 
     @pl.loop(0, n_ep - 1)
     def _(c):

time: 67.8 us -> 66.6 us (0.982)
  Pallas kernels: 65.6 us -> 64.4 us
    pallas_call x1, Pallas kernels: 65.6 us -> 64.4 us  [shards(): pl.pallas_call(functools.partial(layer_kernel, n_ep, n_tp, model_width),...]
where the time goes in v3:
time: 66.6 us; the launch traced here: 66.5 us
  Pallas kernels  64.4 us (97%)
  local copies, waits for them, and re-layouts  2.06 us (3%)
    pallas_call x1, Pallas kernels, shards(): pl.pallas_call(functools.partial(layer_kernel, n_ep, n_tp, model_width),...  64.4 us
    unnamed x1, local copies, waits for them, and re-layouts  2.06 us

profile of v3, /device:TPU:0, one launch (start us, length us, event | category | flops | bytes accessed | tf_op | source)
XLA Modules:
  0.0 66.5 jit_solution(17211306067652606501)
XLA Ops:
  0.0 64.4 %shard_map.82 = bf16[384,1024]{1,0:T(8,128)(2,1)} custom-call(bf16[384,1024]{1,0:T(8,128)(2,1)} %tokens_ref.1, f32[1,4096]{1,0:T(1,128)} %bitcast.2, f32[1,1024]{1,0:T(1,128)} %bitcast.3, s32[1,4,48]{2,1,0:T(4,128)} %chosen_ref.1, f32[1,4,48]{2,1,0:T(4,128)} %weight_ref.1, bf16[1,4096,768]{2,1,0:T(8,128)(2,1)} %gate_hbm.1, bf16[1,4096,768]{2,1,0:T(8,128)(2,1)} %up_hbm.1, ...), custom_call_target="tpu_custom_call" | custom-call | tf_op jit(solution)/shard_map/pallas_call | solution.py:369
  64.4 2.1 %copy.10 = bf16[384,1024]{1,0:T(8,128)(2,1)} copy(bf16[384,1024]{1,0:T(8,128)(2,1)} %shard_map.82) | data formatting | bytes 1572864
